TPU v7x, 32 devices: a whole 2x2x4 slice. The times are simulated.
32 devices in a mesh: grp: 2 (over y), kv: 4 (over z), tp: 4 (over x, core).
Axes of the slice: x: 2, y: 2, z: 4, core: 2. Of those that a mesh axis runs over, the one named last changes fastest.
Arguments:
- tokens: bfloat16 [32, 4096], P('grp', ('kv', 'tp')), parts along dimension 0, may hold values from -50 to 50
- mix_gain: bfloat16 [4096], P('kv'), may hold values from 0.099609375 to 1.8984375
- w_query: bfloat16 [4096, 2048], P('kv', 'tp'), may hold values from -0.09375 to 0.09375
- w_forget: bfloat16 [4096, 2048], P('kv', 'tp'), may hold values from -0.09375 to 0.09375
- w_input: bfloat16 [4096, 2048], P('kv', 'tp'), may hold values from -0.09375 to 0.09375
- w_outgate: bfloat16 [4096, 2048], P('kv', 'tp'), may hold values from -0.09375 to 0.09375
- lower_bound: float32 [2048], P('tp'), may hold values from 0.05 to 0.9
- state: float32 [32, 16, 128, 128], P(('grp', 'kv'), 'tp'), parts along dimension 0, may hold values from -4 to 4
- head_gain: bfloat16 [128], replicated, may hold values from 0.099609375 to 1.8984375
- w_mixout: bfloat16 [2048, 4096], P('tp', 'kv'), may hold values from -0.125 to 0.125
- ffn_gain: bfloat16 [4096], P('kv'), may hold values from 0.099609375 to 1.8984375
- w_gate: bfloat16 [4096, 11264], P('kv', 'tp'), may hold values from -0.09375 to 0.09375
- w_up: bfloat16 [4096, 11264], P('kv', 'tp'), may hold values from -0.09375 to 0.09375
- w_down: bfloat16 [11264, 4096], P('tp', 'kv'), may hold values from -0.0546875 to 0.0546875
Outputs:
- mixed: bfloat16 [32, 4096], P('grp', ('kv', 'tp')), parts along dimension 0
- new_state: float32 [32, 16, 128, 128], P(('grp', 'kv'), 'tp'), parts along dimension 0
There are 2 independent parts, one for each index of `grp`. A program takes and returns all parts, laid end to end along the dimension named above; an argument that names none is the same for every part. Nothing has to cross between parts.
All inputs are finite; a program needn't handle non-finite values.
Results may differ from a plain program's by a relative error of at most 0.01.
Values may be sent and summed in bfloat16 or wider, within the bound.
A program may use at most 64 MiB of HBM per device.

v0:
```python
import jax
import jax.numpy as jnp
from jax import lax
from jax.sharding import PartitionSpec as P

D = 4096


eps = 0.1


def activate(gate_part, up_part, square_sum):
    inv_rms = lax.rsqrt(square_sum / D + eps)[:, None]
    return (jax.nn.silu(gate_part * inv_rms) * (up_part * inv_rms)).astype(jnp.bfloat16)


def body(
    tokens,
    mix_gain,
    w_query,
    w_forget,
    w_input,
    w_outgate,
    lower_bound,
    state,
    head_gain,
    w_mixout,
    ffn_gain,
    w_gate,
    w_up,
    w_down,
):
    rows_here = state.shape[0]
    heads_here = state.shape[1]
    head_size = state.shape[2]
    token_block = lax.all_gather(tokens, "tp", axis=1, tiled=True)
    block_f = token_block.astype(jnp.float32)
    normed = (block_f * mix_gain.astype(jnp.float32)).astype(jnp.bfloat16)
    squares = jnp.sum(block_f * block_f, axis=1)
    query_part = jnp.dot(normed, w_query, preferred_element_type=jnp.float32)
    forget_part = jnp.dot(normed, w_forget, preferred_element_type=jnp.float32)
    input_part = jnp.dot(normed, w_input, preferred_element_type=jnp.float32)
    gate_part = jnp.dot(normed, w_outgate, preferred_element_type=jnp.float32)
    query_raw, forget_raw, input_raw, gate_raw, square_sum = (
        lax.psum_scatter(query_part, "kv", scatter_dimension=0, tiled=True),
        lax.psum_scatter(forget_part, "kv", scatter_dimension=0, tiled=True),
        lax.psum_scatter(input_part, "kv", scatter_dimension=0, tiled=True),
        lax.psum_scatter(gate_part, "kv", scatter_dimension=0, tiled=True),
        lax.psum_scatter(squares, "kv", scatter_dimension=0, tiled=True),
    )
    inv_rms = lax.rsqrt(square_sum / D + eps)[:, None]

    def heads_of(values_raw):
        return (values_raw * inv_rms).reshape(rows_here, heads_here, head_size)

    query_act = jax.nn.silu(heads_of(query_raw))
    forget_pre = heads_of(forget_raw)
    values_in = heads_of(input_raw)
    bounds = lower_bound.reshape(heads_here, head_size)
    forget = bounds + (1.0 - bounds) * jax.nn.sigmoid(forget_pre)
    key_in = (1.0 - bounds) * jax.nn.sigmoid(-forget_pre)
    new_state = forget[..., None] * state + key_in[..., None] * values_in[:, :, None, :]
    readout = jnp.sum(query_act[..., None] * new_state, axis=2)
    head_rms = lax.rsqrt(jnp.mean(readout * readout, axis=-1, keepdims=True) + eps)
    gated_out = readout * head_rms * head_gain.astype(jnp.float32) * jax.nn.silu(heads_of(gate_raw))
    gated_out = gated_out.reshape(rows_here, heads_here * head_size).astype(jnp.bfloat16)
    mix_terms = jnp.dot(
        lax.all_gather(gated_out, "kv", axis=0, tiled=True),
        w_mixout,
        preferred_element_type=jnp.float32,
    )
    mix_own = lax.psum_scatter(mix_terms, "tp", scatter_dimension=1, tiled=True)
    resid_own = (tokens.astype(jnp.float32) + mix_own).astype(jnp.bfloat16)
    resid_block = lax.all_gather(resid_own, "tp", axis=1, tiled=True)
    resid_f = resid_block.astype(jnp.float32)
    normed_ffn = (resid_f * ffn_gain.astype(jnp.float32)).astype(jnp.bfloat16)
    squares_ffn = jnp.sum(resid_f * resid_f, axis=1)
    gate_terms = jnp.dot(normed_ffn, w_gate, preferred_element_type=jnp.float32)
    up_terms = jnp.dot(normed_ffn, w_up, preferred_element_type=jnp.float32)
    gate_total, up_total, square_total = lax.psum((gate_terms, up_terms, squares_ffn), "kv")
    hidden_all = activate(gate_total, up_total, square_total)
    down_terms = jnp.dot(hidden_all, w_down, preferred_element_type=jnp.float32)
    down_own = lax.psum_scatter(down_terms, "tp", scatter_dimension=1, tiled=True)
    mixed = (resid_own.astype(jnp.float32) + down_own).astype(jnp.bfloat16)
    return (mixed, new_state)


def solution(mesh):
    return jax.shard_map(
        body,
        mesh=mesh,
        in_specs=(
            P("grp", ("kv", "tp")),
            P("kv"),
            P("kv", "tp"),
            P("kv", "tp"),
            P("kv", "tp"),
            P("kv", "tp"),
            P("tp"),
            P(("grp", "kv"), "tp", None, None),
            P(),
            P("tp", "kv"),
            P("kv"),
            P("kv", "tp"),
            P("kv", "tp"),
            P("tp", "kv"),
        ),
        out_specs=(P("grp", ("kv", "tp")), P(("grp", "kv"), "tp", None, None)),
        check_vma=False,
    )
```

profile of v0, /device:TPU:0, one launch (start us, length us, event | category | flops | bytes accessed | tf_op | source)
XLA Modules:
  0.0 180.7 jit_solution(14261515714784140611)
XLA Ops:
  7.2 0.8 convert_element_type.41
  8.0 6.4 %all_gather.9 = bf16[16,1024]{1,0:T(8,128)(2,1)S(1)} all-gather(bf16[16,256]{1,0:T(8,128)(2,1)} %param.14), channel_id=1, replica_groups=mesh['grp'=2,'kv'=4,'tp'=4] {'tp'}, dimensions={1}, use_global_device_ids=true | all-gather | bytes 40960 | tf_op jit(solution)/shard_map/all_gather | solution.py:36
  15.1 2.1 %fusion.15 = f32[16,512]{1,0:T(8,128)} fusion(bf16[1024,512]{1,0:T(8,128)(2,1)} %param.17, bf16[16,1024]{1,0:T(8,128)(2,1)S(1)} %all_gather.9, f32[1024]{0:T(1024)S(1)} %convert_element_type.41), kind=kOutput, calls=%fused_computation.20 | convolution fusion | flops 16826368 | bytes 1118208 | tf_op jit(solution)/shard_map/dot_general | solution.py:41
  17.2 2.1 %fusion.13 = f32[16,512]{1,0:T(8,128)} fusion(bf16[1024,512]{1,0:T(8,128)(2,1)} %param.18, bf16[16,1024]{1,0:T(8,128)(2,1)S(1)} %all_gather.9, f32[1024]{0:T(1024)S(1)} %convert_element_type.41), kind=kOutput, calls=%fused_computation.19 | convolution fusion | flops 16826368 | bytes 1118208 | tf_op jit(solution)/shard_map/dot_general | solution.py:42
  19.2 2.1 %fusion.11 = f32[16,512]{1,0:T(8,128)} fusion(bf16[1024,512]{1,0:T(8,128)(2,1)} %param.19, bf16[16,1024]{1,0:T(8,128)(2,1)S(1)} %all_gather.9, f32[1024]{0:T(1024)S(1)} %convert_element_type.41), kind=kOutput, calls=%fused_computation.18 | convolution fusion | flops 16826368 | bytes 1118208 | tf_op jit(solution)/shard_map/dot_general | solution.py:43
  21.3 2.1 %fusion.17 = f32[16,512]{1,0:T(8,128)} fusion(bf16[1024,512]{1,0:T(8,128)(2,1)} %param.16, bf16[16,1024]{1,0:T(8,128)(2,1)S(1)} %all_gather.9, f32[1024]{0:T(1024)S(1)} %convert_element_type.41), kind=kOutput, calls=%fused_computation.21 | convolution fusion | flops 16826368 | bytes 1118208 | tf_op jit(solution)/shard_map/dot_general | solution.py:40
  24.8 1.3 dynamic-slice
  26.7 33.5 %all-reduce.10.cloned.1.call-done = (f32[16]{0:T(128)}, f32[16,512]{1,0:T(8,128)}, f32[16,512]{1,0:T(8,128)}, f32[16,512]{1,0:T(8,128)}, f32[16,512]{1,0:T(8,128)}) async-done(((f32[16]{0:T(128)}, f32[16,512]{1,0:T(8,128)}, f32[16,512]{1,0:T(8,128)}, f32[16,512]{1,0:T(8,128)}, f32[16,512]{1,0:T(8,128)}), (f32[16]{0:T(128)}, f32[16,512]{1,0:T(8,128)}, f32[16,512]{1,0:T(8,128)}, f32[16,512]{1,0:T(8,128)}, ...) | async-done | bytes 131152
  60.9 0.8 add_divide_fusion.1
  61.8 0.7 multiply_add_fusion.1
  62.5 2.8 %multiply_reduce_fusion = (f32[4,4,128]{2,1,0:T(4,128)S(1)}, f32[4,4,128,128]{3,2,1,0:T(8,128)}) fusion(f32[4,4,128]{2,1,0:T(4,128)S(1)} %get-tuple-element.17, f32[4,4,128]{2,1,0:T(4,128)S(1)} %mul.181, f32[4,4,128]{2,1,0:T(4,128)S(1)} %get-tuple-element.14, f32[4,4,128,128]{3,2,1,0:T(8,128)} %param.21, f32[4,4,128]{2,1,0:T(4,128)S(1)} %get-tuple-element.13), kind=kLoop, calls=%fused_computation | loop fusion | flops 1308672 | bytes 2138112 | tf_op jit(solution)/shard_map/reduce_sum | solution.py:63
  65.5 0.8 fusion.21
  66.3 13.3 %all-gather = bf16[4,4,512]{2,1,0:T(4,128)(2,1)S(1)} all-gather(bf16[1,4,512]{2,1,0:T(4,128)(2,1)S(1)} %fusion.21), channel_id=1, replica_groups=mesh['grp'=2,'kv'=4,'tp'=4] {'kv'}, dimensions={0}, use_global_device_ids=true | all-gather | bytes 20480 | tf_op jit(solution)/shard_map/all_gather | solution.py:68
  79.6 0.9 fusion.25
  80.6 19.7 %reduce-scatter.3.cloned.1.call-done = f32[16,256]{1,0:T(8,128)} async-done(((f32[16,1024]{1,0:T(8,128)}), f32[16,256]{1,0:T(8,128)}) %reduce-scatter.3.cloned.1.call-update) | async-done | bytes 16400 | tf_op jit(solution)/shard_map/reduce_scatter | solution.py:72
  100.3 0.9 add_convert_fusion.1
  101.1 5.3 %all_gather.11 = bf16[16,1024]{1,0:T(8,128)(2,1)S(1)} all-gather(bf16[16,256]{1,0:T(8,128)(2,1)S(1)} %add_convert_fusion.1), channel_id=1, replica_groups=mesh['grp'=2,'kv'=4,'tp'=4] {'tp'}, dimensions={1}, use_global_device_ids=true | all-gather | bytes 40960 | tf_op jit(solution)/shard_map/all_gather | solution.py:74
  106.4 4.2 %fusion.7 = f32[16,2816]{1,0:T(8,128)} fusion(bf16[1024,2816]{1,0:T(8,128)(2,1)} %param.26, bf16[16,1024]{1,0:T(8,128)(2,1)S(1)} %all_gather.11, f32[1024]{0:T(1024)S(1)} %convert_element_type.48), kind=kOutput, calls=%fused_computation.14 | convolution fusion | flops 92323840 | bytes 5984256 | tf_op jit(solution)/shard_map/dot_general | solution.py:79
  110.6 1.5 fusion.9
  112.3 11.7 %psum.22 = f32[16]{0:T(128)S(1)} all-reduce(f32[16]{0:T(128)S(1)} %fusion.6), channel_id=1, replica_groups=mesh['grp'=2,'kv'=4,'tp'=4] {'kv'}, use_global_device_ids=true, to_apply=%region_11.12 | all-reduce | flops 16 | bytes 128 | tf_op jit(solution)/shard_map/psum | solution.py:80
  124.0 24.9 %all-reduce.12.cloned.1.call-done = (f32[16,2816]{1,0:T(8,128)}, f32[16,2816]{1,0:T(8,128)}) async-done(((f32[16,2816]{1,0:T(8,128)}, f32[16,2816]{1,0:T(8,128)}), (f32[16,2816]{1,0:T(8,128)}, f32[16,2816]{1,0:T(8,128)})) %all-reduce.12.cloned.1.call-update) | async-done | bytes 360464 | tf_op jit(solution)/shard_map/psum | solution.py:80
  149.0 4.4 %fusion = f32[16,1024]{1,0:T(8,128)} fusion(bf16[2816,1024]{1,0:T(8,128)(2,1)} %param.27, f32[16,2816]{1,0:T(8,128)} %get-tuple-element.7, f32[16,2816]{1,0:T(8,128)} %get-tuple-element.8, f32[16]{0:T(128)S(1)} %add_rsqrt_fusion.1), kind=kOutput, calls=%fused_computation.3 | convolution fusion | flops 92635136 | bytes 6193216 | tf_op jit(solution)/shard_map/dot_general | solution.py:82
  153.4 19.5 %reduce-scatter.5.cloned.1.call-done = f32[16,256]{1,0:T(8,128)} async-done(((f32[16,1024]{1,0:T(8,128)}), f32[16,256]{1,0:T(8,128)}) %reduce-scatter.5.cloned.1.call-update) | async-done | bytes 16400 | tf_op jit(solution)/shard_map/reduce_scatter | solution.py:83
  172.9 1.3 add_convert_fusion
  (32 shorter events, 3.3 us)
Async XLA Ops:
  7.2 72.4 %copy-start = (bf16[512,1024]{1,0:T(8,128)(2,1)S(1)}, bf16[512,1024]{1,0:T(8,128)(2,1)}, u32[]{:S(2)}) copy-start(bf16[512,1024]{1,0:T(8,128)(2,1)} %param.23) | copy-start | bytes 3145732
  7.2 93.1 %copy-start.2 = (bf16[16,256]{1,0:T(8,128)(2,1)S(1)}, bf16[16,256]{1,0:T(8,128)(2,1)}, u32[]{:S(2)}) copy-start(bf16[16,256]{1,0:T(8,128)(2,1)} %param.14) | copy-start | bytes 24580
  7.2 73.4 %copy-start.3 = (bf16[1024]{0:T(1024)(128)(2,1)S(1)}, bf16[1024]{0:T(1024)(128)(2,1)}, u32[]{:S(2)}) copy-start(bf16[1024]{0:T(1024)(128)(2,1)} %param.24) | copy-start | bytes 6148
  7.2 53.0 %all-reduce.10.cloned.1.call-start = ((), (), s32[]{:S(2)}) async-start(), calls=%async_computation.4 | async-start | bytes 263168
  23.4 76.8 %reduce-scatter.3.cloned.1.call-start = ((), (), s32[]{:S(2)}) async-start(), calls=%async_computation.2 | async-start | bytes 81920 | tf_op jit(solution)/shard_map/reduce_scatter | solution.py:72
  80.5 68.5 %all-reduce.12.cloned.1.call-start = ((), (), s32[]{:S(2)}) async-start(), calls=%async_computation.5 | async-start | bytes 720896 | tf_op jit(solution)/shard_map/psum | solution.py:80
  100.3 10.3 %copy-start.1 = (bf16[1024,2816]{1,0:T(8,128)(2,1)S(1)}, bf16[1024,2816]{1,0:T(8,128)(2,1)}, u32[]{:S(2)}) copy-start(bf16[1024,2816]{1,0:T(8,128)(2,1)} %param.25) | copy-start | bytes 17301508
  112.2 60.7 %reduce-scatter.5.cloned.1.call-start = ((), (), s32[]{:S(2)}) async-start(), calls=%async_computation.3 | async-start | bytes 81920 | tf_op jit(solution)/shard_map/reduce_scatter | solution.py:83
Sparse Core Ops, SparseCore 0:
  23.5 36.6 all-reduce.9
  80.6 19.5 reduce-scatter.2
  112.3 36.6 all-reduce.11
  153.5 19.3 reduce-scatter.4
where the time goes:
time: 181 us
  waiting for transfers between devices  97.7 us (54%)
  blocking collectives  36.7 us (20%)
  matrix products  19.3 us (11%)
  between operations  14.5 us (8%)
  other arithmetic  11.1 us (6%)
    unnamed x5, waiting for transfers between devices  33.6 us
    psum x1, waiting for transfers between devices, body(): lax.psum((gate_terms, up_terms, squares_ffn), 'kv')  24.9 us
    reduce_scatter x1, waiting for transfers between devices, body(): mix_own = lax.psum_scatter(mix_terms, 'tp', scatter_dimension=1, tiled=True)  19.7 us
    reduce_scatter x1, waiting for transfers between devices, body(): lax.psum_scatter(down_terms, 'tp', scatter_dimension=1, tiled=True)  19.5 us
    all_gather x1, blocking collectives, body(): lax.all_gather(gated_out, 'kv', axis=0, tiled=True)  13.3 us
    psum x1, blocking collectives, body(): lax.psum((gate_terms, up_terms, squares_ffn), 'kv')  11.7 us
    all_gather x1, blocking collectives, body(): token_block = lax.all_gather(tokens, 'tp', axis=1, tiled=True)  6.44 us
    all_gather x1, blocking collectives, body(): resid_block = lax.all_gather(resid_own, 'tp', axis=1, tiled=True)  5.3 us
  transfers between devices with their start and end apart: 4, of which 4 were waited for; matrix products, arithmetic and copies ran while one was open for 2% of the time, Pallas kernels for 0%

commit v1 on v0

v1 whole, which is shorter than its diff:
```python
import functools

import jax
import jax.numpy as jnp
from jax import lax
from jax.experimental import pallas as pl
from jax.experimental.pallas import tpu as pltpu
from jax.sharding import PartitionSpec as P

eps = 0.1
LANES = 128
F32 = jnp.float32
BF16 = jnp.bfloat16


def split_squares(squares):
    wide = jnp.broadcast_to(squares, (squares.shape[0], LANES))
    high = wide.astype(BF16).astype(F32)
    lane = lax.broadcasted_iota(jnp.int32, wide.shape, 1)
    return jnp.where(lane < LANES // 2, high, wide - high)


def join_squares(tile):
    return tile[:, :1] + tile[:, LANES // 2 : LANES // 2 + 1]


def kernel(
    n_kv,
    n_tp,
    tokens,
    mix_gain,
    w_query,
    w_forget,
    w_input,
    w_outgate,
    lower_bound,
    state,
    head_gain,
    w_mixout,
    ffn_gain,
    w_gate,
    w_up,
    w_down,
    mixed,
    new_state,
    proj_v,
    state_v,
    mixout_v,
    gate_v,
    up_v,
    down_v,
    next_v,
    tok_buf,
    proj_f,
    proj_send,
    proj_recv,
    read_buf,
    read_f,
    mix_buf,
    resid_buf,
    ffn_f,
    ffn_send,
    ffn_recv,
    hid_buf,
    hid_f,
    down_send,
    down_recv,
    load_sem,
    tok_s,
    tok_r,
    proj_s,
    proj_r,
    read_s,
    read_r,
    mix_s,
    mix_r,
    ffn_s,
    ffn_r,
    hid_s,
    hid_r,
    down_s,
    down_r,
):
    kv = lax.axis_index("kv")
    tp = lax.axis_index("tp")
    rows, heads, size, _ = state.shape
    width = w_query.shape[1]
    hidden = w_gate.shape[1]
    cols = tokens.shape[1]
    model = w_query.shape[0] * n_kv

    loads = [
        pltpu.make_async_copy(src, dst, load_sem.at[i])
        for i, (src, dst) in enumerate(
            [
                (tokens, tok_buf.at[tp]),
                (w_query, proj_v.at[0]),
                (w_forget, proj_v.at[1]),
                (w_input, proj_v.at[2]),
                (w_outgate, proj_v.at[3]),
                (state, state_v),
                (w_mixout, mixout_v),
                (w_gate, gate_v),
                (w_up, up_v),
                (w_down, down_v),
            ]
        )
    ]
    for load in loads:
        load.start()

    barrier = pltpu.get_barrier_semaphore()
    for d in range(1, n_tp):
        pl.semaphore_signal(barrier, inc=1, device_id={"tp": lax.rem(tp + d, n_tp)})
    for d in range(1, n_kv):
        pl.semaphore_signal(barrier, inc=1, device_id={"kv": lax.rem(kv + d, n_kv)})
    pl.semaphore_wait(barrier, n_tp - 1 + n_kv - 1)

    sent = []

    def exchange(axis, me, n, source, target, send_sem, recv_sem):
        copies = []
        for d in reversed(range(1, n)):
            peer = lax.rem(me + d, n)
            copy = pltpu.make_async_remote_copy(
                src_ref=source(peer),
                dst_ref=target(d),
                send_sem=send_sem.at[d - 1],
                recv_sem=recv_sem.at[d - 1],
                device_id={axis: peer},
            )
            copy.start()
            copies.append(copy)
        sent.extend(copies)
        return copies

    loads[0].wait()
    own = tok_buf.at[tp]
    for copy in exchange("tp", tp, n_tp, lambda p: own, lambda d: own, tok_s, tok_r):
        copy.wait_recv()
    block = jnp.concatenate([tok_buf[i].astype(F32) for i in range(n_tp)], axis=1)
    normed = (block * mix_gain[...].astype(F32)).astype(BF16)
    proj_f[:, 4 * width :] = split_squares(jnp.sum(block * block, axis=1, keepdims=True))

    for i in range(4):
        loads[1 + i].wait()
        proj_f[:, i * width : (i + 1) * width] = jnp.dot(
            normed, proj_v[i], preferred_element_type=F32
        )
    for j in range(n_kv):
        proj_send[j] = proj_f[j * rows : (j + 1) * rows, :].astype(BF16)
    copies = exchange(
        "kv", kv, n_kv, lambda p: proj_send.at[p], lambda d: proj_recv.at[d - 1], proj_s, proj_r
    )
    total = proj_send[kv].astype(F32)
    loads[5].wait()
    for d, copy in zip(reversed(range(1, n_kv)), copies):
        copy.wait_recv()
        total += proj_recv[d - 1].astype(F32)

    inv_rms = lax.rsqrt(join_squares(total[:, 4 * width :]) / model + eps)
    query_raw, forget_raw, input_raw, gate_raw = (
        total[:, i * width : (i + 1) * width] * inv_rms for i in range(4)
    )
    bounds = lower_bound[...]
    forget = bounds + (1.0 - bounds) * jax.nn.sigmoid(forget_raw)
    key_in = (1.0 - bounds) * jax.nn.sigmoid(-forget_raw)
    query_act = query_raw * jax.nn.sigmoid(query_raw)
    gate_act = gate_raw * jax.nn.sigmoid(gate_raw)
    gain = head_gain[...].astype(F32)
    pad = jnp.zeros((-(3 * rows) % 8, width), F32)
    turned = jnp.concatenate([forget, key_in, query_act, pad], axis=0).T
    pieces = []
    for h in range(heads):
        here = slice(h * size, (h + 1) * size)
        readouts = []
        for b in range(rows):
            forget_c = turned[here, b : b + 1]
            key_c = turned[here, rows + b : rows + b + 1]
            query_c = turned[here, 2 * rows + b : 2 * rows + b + 1]
            after = forget_c * state_v[b, h] + key_c * input_raw[b : b + 1, here]
            next_v[b, h] = after
            readouts.append(jnp.sum(query_c * after, axis=0, keepdims=True))
        readout = jnp.concatenate(readouts, axis=0)
        head_rms = lax.rsqrt(jnp.mean(readout * readout, axis=1, keepdims=True) + eps)
        pieces.append(readout * head_rms * gain * gate_act[:, here])
    read_buf[kv] = jnp.concatenate(pieces, axis=1).astype(BF16)
    own_read = read_buf.at[kv]
    copies = exchange("kv", kv, n_kv, lambda p: own_read, lambda d: own_read, read_s, read_r)
    store = pltpu.make_async_copy(next_v, new_state, load_sem.at[len(loads)])
    store.start()
    loads[6].wait()
    for copy in copies:
        copy.wait_recv()
    for j in range(n_kv):
        read_f[j * rows : (j + 1) * rows, :] = read_buf[j].astype(F32)

    mix_buf[tp] = jnp.dot(
        read_f[...].astype(BF16), mixout_v[...], preferred_element_type=F32
    ).astype(BF16)
    own_mix = mix_buf.at[tp]
    copies = exchange("tp", tp, n_tp, lambda p: own_mix, lambda d: own_mix, mix_s, mix_r)
    for copy in copies:
        copy.wait_recv()
    mix_sum = mix_buf[0].astype(F32)
    for i in range(1, n_tp):
        mix_sum += mix_buf[i].astype(F32)
    resid = (block + mix_sum).astype(BF16).astype(F32)
    for i in range(n_tp):
        resid_buf[i] = resid[:, i * cols : (i + 1) * cols]
    normed_ffn = (resid * ffn_gain[...].astype(F32)).astype(BF16)
    ffn_f[:, 2 * hidden :] = split_squares(jnp.sum(resid * resid, axis=1, keepdims=True))

    loads[7].wait()
    ffn_f[:, :hidden] = jnp.dot(normed_ffn, gate_v[...], preferred_element_type=F32)
    loads[8].wait()
    ffn_f[:, hidden : 2 * hidden] = jnp.dot(normed_ffn, up_v[...], preferred_element_type=F32)
    for j in range(n_kv):
        ffn_send[j] = ffn_f[j * rows : (j + 1) * rows, :].astype(BF16)
    copies = exchange(
        "kv", kv, n_kv, lambda p: ffn_send.at[p], lambda d: ffn_recv.at[d - 1], ffn_s, ffn_r
    )
    total = ffn_send[kv].astype(F32)
    for d, copy in zip(reversed(range(1, n_kv)), copies):
        copy.wait_recv()
        total += ffn_recv[d - 1].astype(F32)
    inv_rms = lax.rsqrt(join_squares(total[:, 2 * hidden :]) / model + eps)
    gate_sum = total[:, :hidden] * inv_rms
    up_sum = total[:, hidden : 2 * hidden] * inv_rms
    hid_buf[kv] = (gate_sum * jax.nn.sigmoid(gate_sum) * up_sum).astype(BF16)
    own_hid = hid_buf.at[kv]
    copies = exchange("kv", kv, n_kv, lambda p: own_hid, lambda d: own_hid, hid_s, hid_r)
    loads[9].wait()
    for copy in copies:
        copy.wait_recv()
    for j in range(n_kv):
        hid_f[j * rows : (j + 1) * rows, :] = hid_buf[j].astype(F32)

    down = jnp.dot(hid_f[...].astype(BF16), down_v[...], preferred_element_type=F32)
    for i in range(n_tp):
        down_send[i] = down[:, i * cols : (i + 1) * cols].astype(BF16)
    copies = exchange(
        "tp", tp, n_tp, lambda p: down_send.at[p], lambda d: down_recv.at[d - 1], down_s, down_r
    )
    result = down_send[tp].astype(F32)
    for d, copy in zip(reversed(range(1, n_tp)), copies):
        copy.wait_recv()
        result += down_recv[d - 1].astype(F32)
    mixed[...] = (resid_buf[tp] + result).astype(BF16)

    for copy in sent:
        copy.wait_send()
    store.wait()


def body(n_kv, n_tp, *args):
    (
        tokens,
        mix_gain,
        w_query,
        w_forget,
        w_input,
        w_outgate,
        lower_bound,
        state,
        head_gain,
        w_mixout,
        ffn_gain,
        w_gate,
        w_up,
        w_down,
    ) = args
    batch, cols = tokens.shape
    block, width = w_query.shape
    rows = state.shape[0]
    hidden = w_gate.shape[1]
    any_spec = pl.BlockSpec(memory_space=pl.ANY)
    vmem = pl.BlockSpec(memory_space=pltpu.VMEM)
    sems = [pltpu.SemaphoreType.DMA((16,))]
    for n in (n_tp, n_kv, n_kv, n_tp, n_kv, n_kv, n_tp):
        sems += [pltpu.SemaphoreType.DMA((max(n - 1, 1),))] * 2
    return pl.pallas_call(
        functools.partial(kernel, n_kv, n_tp),
        out_shape=(
            jax.ShapeDtypeStruct(tokens.shape, BF16),
            jax.ShapeDtypeStruct(state.shape, F32),
        ),
        in_specs=[
            any_spec,
            vmem,
            any_spec,
            any_spec,
            any_spec,
            any_spec,
            vmem,
            any_spec,
            vmem,
            any_spec,
            vmem,
            any_spec,
            any_spec,
            any_spec,
        ],
        out_specs=(vmem, any_spec),
        scratch_shapes=[
            pltpu.VMEM((4, block, width), BF16),
            pltpu.VMEM(state.shape, F32),
            pltpu.VMEM(w_mixout.shape, BF16),
            pltpu.VMEM(w_gate.shape, BF16),
            pltpu.VMEM(w_up.shape, BF16),
            pltpu.VMEM(w_down.shape, BF16),
            pltpu.VMEM(state.shape, F32),
            pltpu.VMEM((n_tp, batch, cols), BF16),
            pltpu.VMEM((batch, 4 * width + LANES), F32),
            pltpu.VMEM((n_kv, rows, 4 * width + LANES), BF16),
            pltpu.VMEM((n_kv, rows, 4 * width + LANES), BF16),
            pltpu.VMEM((n_kv, rows, width), BF16),
            pltpu.VMEM((batch, width), F32),
            pltpu.VMEM((n_tp, batch, block), BF16),
            pltpu.VMEM((n_tp, batch, cols), F32),
            pltpu.VMEM((batch, 2 * hidden + LANES), F32),
            pltpu.VMEM((n_kv, rows, 2 * hidden + LANES), BF16),
            pltpu.VMEM((n_kv, rows, 2 * hidden + LANES), BF16),
            pltpu.VMEM((n_kv, rows, hidden), BF16),
            pltpu.VMEM((batch, hidden), F32),
            pltpu.VMEM((n_tp, batch, cols), BF16),
            pltpu.VMEM((n_tp, batch, cols), BF16),
            *sems,
        ],
        compiler_params=pltpu.CompilerParams(collective_id=0, has_side_effects=True),
    )(
        tokens,
        mix_gain.reshape(1, -1),
        w_query,
        w_forget,
        w_input,
        w_outgate,
        lower_bound.reshape(1, -1),
        state,
        head_gain.reshape(1, -1),
        w_mixout,
        ffn_gain.reshape(1, -1),
        w_gate,
        w_up,
        w_down,
    )


def solution(mesh):
    return jax.shard_map(
        functools.partial(body, mesh.shape["kv"], mesh.shape["tp"]),
        mesh=mesh,
        in_specs=(
            P("grp", ("kv", "tp")),
            P("kv"),
            P("kv", "tp"),
            P("kv", "tp"),
            P("kv", "tp"),
            P("kv", "tp"),
            P("tp"),
            P(("grp", "kv"), "tp", None, None),
            P(),
            P("tp", "kv"),
            P("kv"),
            P("kv", "tp"),
            P("kv", "tp"),
            P("tp", "kv"),
        ),
        out_specs=(P("grp", ("kv", "tp")), P(("grp", "kv"), "tp", None, None)),
        check_vma=False,
    )
```

time: 181 us -> 45.4 us (0.25)
  waiting for transfers between devices: 97.7 us -> 0 us
  Pallas kernels: 0 us -> 38.3 us
  blocking collectives: 36.7 us -> 0 us
  matrix products: 19.3 us -> 0 us
  between operations: 14.5 us -> 0.64 us
  other arithmetic: 11.1 us -> 0 us
  local copies, waits for them, and re-layouts: 1.37 us -> 6.15 us
    reduce_scatter x2 -> x0, waiting for transfers between devices: 39.2 us -> none  [the longest x1 19.7 us: body(): mix_own = lax.psum_scatter(mix_terms, 'tp', scatter_dimension=1, tiled=True)]
    pallas_call x0 -> x1, Pallas kernels: none -> 38.3 us  [body(): pl.pallas_call(functools.partial(kernel, n_kv, n_tp), out_shape=(jax.Shap...]
    unnamed x5 -> x0, waiting for transfers between devices: 33.6 us -> none
    all_gather x3 -> x0, blocking collectives: 25 us -> none  [the longest x1 13.3 us: body(): lax.all_gather(gated_out, 'kv', axis=0, tiled=True)]
    psum x1 -> x0, waiting for transfers between devices: 24.9 us -> none  [body(): lax.psum((gate_terms, up_terms, squares_ffn), 'kv')]
    dot_general x8 -> x0, matrix products: 19.3 us -> none  [the longest x1 4.37 us: body(): down_terms = jnp.dot(hidden_all, w_down, preferred_element_type=jnp.float32)]
    psum x1 -> x0, blocking collectives: 11.7 us -> none  [body(): lax.psum((gate_terms, up_terms, squares_ffn), 'kv')]
    reduce_sum x4 -> x0, other arithmetic: 3.64 us -> none  [the longest x1 2.8 us: body(): readout = jnp.sum(query_act[..., None] * new_state, axis=2)]
  transfers between devices with their start and end apart: 4 -> 0, of which waited for: 4 -> 0; matrix products, arithmetic and copies ran while one was open for 2% -> 0% of each run, Pallas kernels for 0% -> 0%
where the time goes in v1:
time: 45.4 us; the launch traced here: 45.1 us
  Pallas kernels  38.3 us (84%)
  local copies, waits for them, and re-layouts  6.15 us (14%)
  between operations  0.64 us (1%)
    pallas_call x1, Pallas kernels, body(): pl.pallas_call(functools.partial(kernel, n_kv, n_tp), out_shape=(jax.Shap...  38.3 us
    unnamed x2, local copies, waits for them, and re-layouts  3.59 us
    reshape x1, local copies, waits for them, and re-layouts, body(): mix_gain.reshape(1, -1)  1.28 us
    reshape x1, local copies, waits for them, and re-layouts, body(): ffn_gain.reshape(1, -1)  1.28 us

profile of v1, /device:TPU:0, one launch (start us, length us, event | category | flops | bytes accessed | tf_op | source)
XLA Modules:
  0.0 45.1 jit_solution(1874013451250257778)
XLA Ops:
  0.6 1.3 %reshape.16.mix_gain = bf16[1,1024]{1,0:T(2,128)(2,1)} reshape(bf16[1024]{0:T(1024)(128)(2,1)} %param.15) | data formatting | bytes 4096 | tf_op jit(solution)/shard_map/reshape | solution.py:333
  1.9 1.3 %reshape.19.ffn_gain = bf16[1,1024]{1,0:T(2,128)(2,1)} reshape(bf16[1024]{0:T(1024)(128)(2,1)} %param.24) | data formatting | bytes 4096 | tf_op jit(solution)/shard_map/reshape | solution.py:342
  3.2 38.3 %shard_map.149 = (bf16[16,256]{1,0:T(8,128)(2,1)}, f32[4,4,128,128]{3,2,1,0:T(8,128)}) custom-call(bf16[16,256]{1,0:T(8,128)(2,1)} %tokens.1, bf16[1,1024]{1,0:T(2,128)(2,1)} %reshape.16.mix_gain, bf16[1024,512]{1,0:T(8,128)(2,1)} %w_query.1, bf16[1024,512]{1,0:T(8,128)(2,1)} %w_forget.1, bf16[1024,512]{1,0:T(8,128)(2,1)} %w_input.1, ...), custom_call_target="tpu_custom_call" | custom-call | tf_op jit(solution)/shard_map/pallas_call | solution.py:282
  41.5 1.3 %copy.18 = bf16[16,256]{1,0:T(8,128)(2,1)} copy(bf16[16,256]{1,0:T(8,128)(2,1)} %get-tuple-element.4) | data formatting | bytes 16384
  42.8 2.3 %copy.19 = f32[4,4,128,128]{3,2,1,0:T(8,128)} copy(f32[4,4,128,128]{3,2,1,0:T(8,128)} %get-tuple-element.5) | data formatting | bytes 2097152

commit v2 on v1

v2 whole, which is shorter than its diff:
```python
import functools

import jax
import jax.numpy as jnp
from jax import lax
from jax.experimental import pallas as pl
from jax.experimental.pallas import tpu as pltpu
from jax.sharding import PartitionSpec as P

eps = 0.1
LANES = 128
CHUNKS = 4
F32 = jnp.float32
BF16 = jnp.bfloat16


def split_squares(squares):
    wide = jnp.broadcast_to(squares, (squares.shape[0], LANES))
    high = wide.astype(BF16).astype(F32)
    lane = lax.broadcasted_iota(jnp.int32, wide.shape, 1)
    return jnp.where(lane < LANES // 2, high, wide - high)


def join_squares(tile):
    return tile[:, :1] + tile[:, LANES // 2 : LANES // 2 + 1]


def row_of(ref):
    wide = ref[...].astype(F32)
    return jnp.concatenate([wide[i : i + 1] for i in range(wide.shape[0])], axis=1)


def tail(mixed_in, state_in, mixed, state, mixed_v, state_v, in_sem, out_sem):
    moves = [(mixed_in, mixed_v, mixed)]
    for i in range(state_v.shape[0]):
        moves.append((state_in.at[i], state_v.at[i], state.at[i]))
    first = [
        pltpu.make_async_copy(src, mid, in_sem.at[i]) for i, (src, mid, _) in enumerate(moves)
    ]
    second = [
        pltpu.make_async_copy(mid, dst, out_sem.at[i]) for i, (_, mid, dst) in enumerate(moves)
    ]
    for copy in first:
        copy.start()
    for one, two in zip(first, second):
        one.wait()
        two.start()
    for copy in second:
        copy.wait()


def kernel(
    n_kv,
    n_tp,
    chunks,
    tokens,
    mix_gain,
    w_query,
    w_forget,
    w_input,
    w_outgate,
    lower_bound,
    state,
    head_gain,
    w_mixout,
    ffn_gain,
    w_gate,
    w_up,
    w_down,
    mixed,
    new_state,
    proj_v,
    state_v,
    mixout_v,
    gate_v,
    up_v,
    down_v,
    next_v,
    mix_gain_v,
    bound_v,
    head_gain_v,
    ffn_gain_v,
    mixed_v,
    tok_buf,
    read_buf,
    read_f,
    mix_buf,
    resid_buf,
    down_send,
    down_recv,
    load_sem,
    store_sem,
    tok_s,
    tok_r,
    proj_s,
    proj_r,
    read_s,
    read_r,
    mix_s,
    mix_r,
    ffn_s,
    ffn_r,
    hid_s,
    hid_r,
    down_s,
    down_r,
    *chunk_bufs,
):
    kv = lax.axis_index("kv")
    tp = lax.axis_index("tp")
    rows, heads, size, _ = state.shape
    width = w_query.shape[1]
    hidden = w_gate.shape[1]
    cols = tokens.shape[1]
    model = w_query.shape[0] * n_kv
    proj_f, proj_send, proj_recv = (chunk_bufs[i : 12 : 3] for i in range(3))
    ffn_f, ffn_send, ffn_recv, hid_buf, hid_f = (chunk_bufs[12 + i :: 5] for i in range(5))

    loads = [
        pltpu.make_async_copy(src, dst, load_sem.at[i])
        for i, (src, dst) in enumerate(
            [
                (tokens, tok_buf.at[tp]),
                (mix_gain, mix_gain_v),
                (w_query, proj_v.at[0]),
                (w_forget, proj_v.at[1]),
                (w_input, proj_v.at[2]),
                (w_outgate, proj_v.at[3]),
                (lower_bound, bound_v),
                (head_gain, head_gain_v),
                (ffn_gain, ffn_gain_v),
                (state, state_v),
                (w_mixout, mixout_v),
                (w_gate, gate_v),
                (w_up, up_v),
                (w_down, down_v),
            ]
        )
    ]
    for load in loads:
        load.start()

    barrier = pltpu.get_barrier_semaphore()
    for d in range(1, n_tp):
        pl.semaphore_signal(barrier, inc=1, device_id={"tp": lax.rem(tp + d, n_tp)})
    for d in range(1, n_kv):
        pl.semaphore_signal(barrier, inc=1, device_id={"kv": lax.rem(kv + d, n_kv)})
    pl.semaphore_wait(barrier, n_tp - 1 + n_kv - 1)

    sent = []

    def exchange(axis, me, n, source, target, send_sem, recv_sem, base=0):
        copies = []
        for d in reversed(range(1, n)):
            peer = lax.rem(me + d, n)
            copy = pltpu.make_async_remote_copy(
                src_ref=source(peer),
                dst_ref=target(d),
                send_sem=send_sem.at[base + d - 1],
                recv_sem=recv_sem.at[base + d - 1],
                device_id={axis: peer},
            )
            copy.start()
            copies.append(copy)
        sent.extend(copies)
        return copies

    loads[0].wait()
    own = tok_buf.at[tp]
    for copy in exchange("tp", tp, n_tp, lambda p: own, lambda d: own, tok_s, tok_r):
        copy.wait_recv()
    loads[1].wait()
    block = jnp.concatenate([tok_buf[i].astype(F32) for i in range(n_tp)], axis=1)
    normed = (block * row_of(mix_gain_v)).astype(BF16)
    proj_f[0][:, width:] = split_squares(jnp.sum(block * block, axis=1, keepdims=True))

    proj_copies = []
    for i in range(4):
        loads[2 + i].wait()
        proj_f[i][:, :width] = jnp.dot(normed, proj_v[i], preferred_element_type=F32)
        send, recv = proj_send[i], proj_recv[i]
        for j in range(n_kv):
            send[j] = proj_f[i][j * rows : (j + 1) * rows, :].astype(BF16)
        proj_copies.append(
            exchange(
                "kv",
                kv,
                n_kv,
                lambda p: send.at[p],
                lambda d: recv.at[d - 1],
                proj_s,
                proj_r,
                i * (n_kv - 1),
            )
        )

    def collect(copies, send, recv):
        total = send[kv].astype(F32)
        for d, copy in zip(reversed(range(1, n_kv)), copies):
            copy.wait_recv()
            total += recv[d - 1].astype(F32)
        return total

    for load in loads[6:10]:
        load.wait()
    totals = [collect(*one) for one in zip(proj_copies, proj_send, proj_recv)]
    inv_rms = lax.rsqrt(join_squares(totals[0][:, width:]) / model + eps)
    query_raw, forget_raw, input_raw, gate_raw = (
        totals[i][:, :width] * inv_rms for i in range(4)
    )
    bounds = row_of(bound_v)
    forget = bounds + (1.0 - bounds) * jax.nn.sigmoid(forget_raw)
    key_in = (1.0 - bounds) * jax.nn.sigmoid(-forget_raw)
    query_act = query_raw * jax.nn.sigmoid(query_raw)
    gate_act = gate_raw * jax.nn.sigmoid(gate_raw)
    gain = row_of(head_gain_v)
    pad = jnp.zeros((-(3 * rows) % 8, width), F32)
    turned = jnp.concatenate([forget, key_in, query_act, pad], axis=0).T
    pieces = []
    for h in range(heads):
        here = slice(h * size, (h + 1) * size)
        readouts = []
        for b in range(rows):
            forget_c = turned[here, b : b + 1]
            key_c = turned[here, rows + b : rows + b + 1]
            query_c = turned[here, 2 * rows + b : 2 * rows + b + 1]
            after = forget_c * state_v[b, h] + key_c * input_raw[b : b + 1, here]
            next_v[b, h] = after
            readouts.append(jnp.sum(query_c * after, axis=0, keepdims=True))
        readout = jnp.concatenate(readouts, axis=0)
        head_rms = lax.rsqrt(jnp.mean(readout * readout, axis=1, keepdims=True) + eps)
        pieces.append(readout * head_rms * gain * gate_act[:, here])
    read_buf[kv] = jnp.concatenate(pieces, axis=1).astype(BF16)
    own_read = read_buf.at[kv]
    copies = exchange("kv", kv, n_kv, lambda p: own_read, lambda d: own_read, read_s, read_r)
    store = pltpu.make_async_copy(next_v, new_state, store_sem.at[0])
    store.start()
    loads[10].wait()
    for copy in copies:
        copy.wait_recv()
    for j in range(n_kv):
        read_f[j * rows : (j + 1) * rows, :] = read_buf[j].astype(F32)

    mix_buf[tp] = jnp.dot(
        read_f[...].astype(BF16), mixout_v[...], preferred_element_type=F32
    ).astype(BF16)
    own_mix = mix_buf.at[tp]
    copies = exchange("tp", tp, n_tp, lambda p: own_mix, lambda d: own_mix, mix_s, mix_r)
    for copy in copies:
        copy.wait_recv()
    mix_sum = mix_buf[0].astype(F32)
    for i in range(1, n_tp):
        mix_sum += mix_buf[i].astype(F32)
    resid = (block + mix_sum).astype(BF16).astype(F32)
    for i in range(n_tp):
        resid_buf[i] = resid[:, i * cols : (i + 1) * cols]
    normed_ffn = (resid * row_of(ffn_gain_v)).astype(BF16)
    ffn_f[0][:, 2 * chunks[0][1] :] = split_squares(jnp.sum(resid * resid, axis=1, keepdims=True))

    loads[11].wait()
    loads[12].wait()
    ffn_copies = []
    for c, (start, count) in enumerate(chunks):
        for i, weight in enumerate((gate_v, up_v)):
            ffn_f[c][:, i * count : (i + 1) * count] = jnp.dot(
                normed_ffn, weight[:, start : start + count], preferred_element_type=F32
            )
        send, recv = ffn_send[c], ffn_recv[c]
        for j in range(n_kv):
            send[j] = ffn_f[c][j * rows : (j + 1) * rows, :].astype(BF16)
        ffn_copies.append(
            exchange(
                "kv",
                kv,
                n_kv,
                lambda p: send.at[p],
                lambda d: recv.at[d - 1],
                ffn_s,
                ffn_r,
                c * (n_kv - 1),
            )
        )
    hid_copies = []
    for c, (start, count) in enumerate(chunks):
        total = collect(ffn_copies[c], ffn_send[c], ffn_recv[c])
        if c == 0:
            inv_rms = lax.rsqrt(join_squares(total[:, 2 * count :]) / model + eps)
        gate_sum = total[:, :count] * inv_rms
        up_sum = total[:, count : 2 * count] * inv_rms
        hid_buf[c][kv] = (gate_sum * jax.nn.sigmoid(gate_sum) * up_sum).astype(BF16)
        own_hid = hid_buf[c].at[kv]
        hid_copies.append(
            exchange(
                "kv",
                kv,
                n_kv,
                lambda p: own_hid,
                lambda d: own_hid,
                hid_s,
                hid_r,
                c * (n_kv - 1),
            )
        )

    loads[13].wait()
    down = None
    for c, (start, count) in enumerate(chunks):
        for copy in hid_copies[c]:
            copy.wait_recv()
        for j in range(n_kv):
            hid_f[c][j * rows : (j + 1) * rows, :] = hid_buf[c][j].astype(F32)
        term = jnp.dot(
            hid_f[c][...].astype(BF16),
            down_v[start : start + count, :],
            preferred_element_type=F32,
        )
        down = term if down is None else down + term
    for i in range(n_tp):
        down_send[i] = down[:, i * cols : (i + 1) * cols].astype(BF16)
    copies = exchange(
        "tp", tp, n_tp, lambda p: down_send.at[p], lambda d: down_recv.at[d - 1], down_s, down_r
    )
    result = down_send[tp].astype(F32)
    for d, copy in zip(reversed(range(1, n_tp)), copies):
        copy.wait_recv()
        result += down_recv[d - 1].astype(F32)
    mixed_v[...] = (resid_buf[tp] + result).astype(BF16)
    last = pltpu.make_async_copy(mixed_v, mixed, store_sem.at[1])
    last.start()

    for copy in sent:
        copy.wait_send()
    store.wait()
    last.wait()


def body(n_kv, n_tp, *args):
    (
        tokens,
        mix_gain,
        w_query,
        w_forget,
        w_input,
        w_outgate,
        lower_bound,
        state,
        head_gain,
        w_mixout,
        ffn_gain,
        w_gate,
        w_up,
        w_down,
    ) = args
    batch, cols = tokens.shape
    block, width = w_query.shape
    rows = state.shape[0]
    hidden = w_gate.shape[1]
    unit = 2 * LANES if hidden % (2 * LANES) == 0 else LANES
    units = hidden // unit
    count = -(-units // min(CHUNKS, units))
    chunks = [
        (i * unit, min(count, units - i) * unit) for i in range(0, units, count)
    ]
    any_spec = pl.BlockSpec(memory_space=pl.ANY)
    sems = [pltpu.SemaphoreType.DMA((14,)), pltpu.SemaphoreType.DMA((2,))]
    for n in (
        n_tp - 1,
        4 * (n_kv - 1),
        n_kv - 1,
        n_tp - 1,
        len(chunks) * (n_kv - 1),
        len(chunks) * (n_kv - 1),
        n_tp - 1,
    ):
        sems += [pltpu.SemaphoreType.DMA((max(n, 1),))] * 2
    bufs = []
    for i in range(4):
        wide = width + (LANES if i == 0 else 0)
        bufs += [
            pltpu.VMEM((batch, wide), F32),
            pltpu.VMEM((n_kv, rows, wide), BF16),
            pltpu.VMEM((n_kv, rows, wide), BF16),
        ]
    for i, (_, count) in enumerate(chunks):
        wide = 2 * count + (LANES if i == 0 else 0)
        bufs += [
            pltpu.VMEM((batch, wide), F32),
            pltpu.VMEM((n_kv, rows, wide), BF16),
            pltpu.VMEM((n_kv, rows, wide), BF16),
            pltpu.VMEM((n_kv, rows, count), BF16),
            pltpu.VMEM((batch, count), F32),
        ]
    small = [x.reshape(-1, LANES) for x in (mix_gain, lower_bound, head_gain, ffn_gain)]
    out_shape = (
        jax.ShapeDtypeStruct(tokens.shape, BF16),
        jax.ShapeDtypeStruct(state.shape, F32),
    )
    results = pl.pallas_call(
        functools.partial(kernel, n_kv, n_tp, chunks),
        out_shape=out_shape,
        in_specs=[any_spec] * 14,
        out_specs=(any_spec, any_spec),
        scratch_shapes=[
            pltpu.VMEM((4, block, width), BF16),
            pltpu.VMEM(state.shape, F32),
            pltpu.VMEM(w_mixout.shape, BF16),
            pltpu.VMEM(w_gate.shape, BF16),
            pltpu.VMEM(w_up.shape, BF16),
            pltpu.VMEM(w_down.shape, BF16),
            pltpu.VMEM(state.shape, F32),
            *[pltpu.VMEM(x.shape, x.dtype) for x in small],
            pltpu.VMEM(tokens.shape, BF16),
            pltpu.VMEM((n_tp, batch, cols), BF16),
            pltpu.VMEM((n_kv, rows, width), BF16),
            pltpu.VMEM((batch, width), F32),
            pltpu.VMEM((n_tp, batch, block), BF16),
            pltpu.VMEM((n_tp, batch, cols), F32),
            pltpu.VMEM((n_tp, batch, cols), BF16),
            pltpu.VMEM((n_tp, batch, cols), BF16),
            *sems,
            *bufs,
        ],
        compiler_params=pltpu.CompilerParams(collective_id=0, has_side_effects=True),
    )(
        tokens,
        small[0],
        w_query,
        w_forget,
        w_input,
        w_outgate,
        small[1],
        state,
        small[2],
        w_mixout,
        small[3],
        w_gate,
        w_up,
        w_down,
    )
    return pl.pallas_call(
        tail,
        out_shape=out_shape,
        in_specs=[any_spec] * 2,
        out_specs=(any_spec, any_spec),
        scratch_shapes=[
            pltpu.VMEM(tokens.shape, BF16),
            pltpu.VMEM(state.shape, F32),
            pltpu.SemaphoreType.DMA((1 + rows,)),
            pltpu.SemaphoreType.DMA((1 + rows,)),
        ],
    )(*results)


def solution(mesh):
    return jax.shard_map(
        functools.partial(body, mesh.shape["kv"], mesh.shape["tp"]),
        mesh=mesh,
        in_specs=(
            P("grp", ("kv", "tp")),
            P("kv"),
            P("kv", "tp"),
            P("kv", "tp"),
            P("kv", "tp"),
            P("kv", "tp"),
            P("tp"),
            P(("grp", "kv"), "tp", None, None),
            P(),
            P("tp", "kv"),
            P("kv"),
            P("kv", "tp"),
            P("kv", "tp"),
            P("tp", "kv"),
        ),
        out_specs=(P("grp", ("kv", "tp")), P(("grp", "kv"), "tp", None, None)),
        check_vma=False,
    )
```

time: 45.4 us -> 39.8 us (0.88)
  local copies, waits for them, and re-layouts: 6.15 us -> 0 us
  Pallas kernels: 38.3 us -> 38.9 us
    unnamed x2 -> x0, local copies, waits for them, and re-layouts: 3.59 us -> none
    reshape x2 -> x0, local copies, waits for them, and re-layouts: 2.55 us -> none  [the longest x1 1.28 us: body(): mix_gain.reshape(1, -1)]
    pallas_call x1 -> x2, Pallas kernels: 38.3 us -> 38.9 us  [the longest x1 36.9 us: body(): pl.pallas_call(functools.partial(kernel, n_kv, n_tp, chunks), out_shape=o...]
where the time goes in v2:
time: 39.8 us; the launch traced here: 39.6 us
  Pallas kernels  38.9 us (98%)
  between operations  0.64 us (2%)
    pallas_call x1, Pallas kernels, body(): pl.pallas_call(functools.partial(kernel, n_kv, n_tp, chunks), out_shape=o...  36.9 us
    pallas_call x1, Pallas kernels, body(): pl.pallas_call(tail, out_shape=out_shape, in_specs=[any_spec] * 2, out_sp...  2.01 us

profile of v2, /device:TPU:0, one launch (start us, length us, event | category | flops | bytes accessed | tf_op | source)
XLA Modules:
  0.0 39.6 jit_solution(10449846785734881876)
XLA Ops:
  0.6 36.9 %shard_map.149 = (bf16[16,256]{1,0:T(8,128)(2,1)}, f32[4,4,128,128]{3,2,1,0:T(8,128)}) custom-call(bf16[16,256]{1,0:T(8,128)(2,1)} %tokens.1, bf16[8,128]{1,0:T(8,128)(2,1)} %bitcast.4, bf16[1024,512]{1,0:T(8,128)(2,1)} %w_query.1, bf16[1024,512]{1,0:T(8,128)(2,1)} %w_forget.1, bf16[1024,512]{1,0:T(8,128)(2,1)} %w_input.1, bf16[1024,512]{1,0:T(8,128)(2,1)} %w_outgate.1, ...), custom_call_target="tpu_custom_call" | custom-call | tf_op jit(solution)/shard_map/pallas_call | solution.py:398
  37.6 2.0 %shard_map.150 = (bf16[16,256]{1,0:T(8,128)(2,1)}, f32[4,4,128,128]{3,2,1,0:T(8,128)}) custom-call(bf16[16,256]{1,0:T(8,128)(2,1)} %get-tuple-element.4.mixed_in, f32[4,4,128,128]{3,2,1,0:T(8,128)} %get-tuple-element.5.state_in), custom_call_target="tpu_custom_call" | custom-call | tf_op jit(solution)/shard_map/pallas_call | solution.py:440

commit v3 on v2

--- a/solution.py
+++ b/solution.py
@@ -30,23 +30,15 @@
     return jnp.concatenate([wide[i : i + 1] for i in range(wide.shape[0])], axis=1)
 
 
-def tail(mixed_in, state_in, mixed, state, mixed_v, state_v, in_sem, out_sem):
-    moves = [(mixed_in, mixed_v, mixed)]
-    for i in range(state_v.shape[0]):
-        moves.append((state_in.at[i], state_v.at[i], state.at[i]))
-    first = [
-        pltpu.make_async_copy(src, mid, in_sem.at[i]) for i, (src, mid, _) in enumerate(moves)
+def tail(mixed_in, state_in, mixed, state, sem):
+    moves = [
+        pltpu.make_async_copy(mixed_in, mixed, sem.at[0]),
+        pltpu.make_async_copy(state_in, state, sem.at[1]),
     ]
-    second = [
-        pltpu.make_async_copy(mid, dst, out_sem.at[i]) for i, (_, mid, dst) in enumerate(moves)
-    ]
-    for copy in first:
-        copy.start()
-    for one, two in zip(first, second):
-        one.wait()
-        two.start()
-    for copy in second:
-        copy.wait()
+    for move in moves:
+        move.start()
+    for move in moves:
+        move.wait()
 
 
 def kernel(
@@ -75,12 +67,10 @@
     gate_v,
     up_v,
     down_v,
-    next_v,
     mix_gain_v,
     bound_v,
     head_gain_v,
     ffn_gain_v,
-    mixed_v,
     tok_buf,
     read_buf,
     read_f,
@@ -89,7 +79,6 @@
     down_send,
     down_recv,
     load_sem,
-    store_sem,
     tok_s,
     tok_r,
     proj_s,
@@ -225,7 +214,7 @@
             key_c = turned[here, rows + b : rows + b + 1]
             query_c = turned[here, 2 * rows + b : 2 * rows + b + 1]
             after = forget_c * state_v[b, h] + key_c * input_raw[b : b + 1, here]
-            next_v[b, h] = after
+            new_state[b, h] = after
             readouts.append(jnp.sum(query_c * after, axis=0, keepdims=True))
         readout = jnp.concatenate(readouts, axis=0)
         head_rms = lax.rsqrt(jnp.mean(readout * readout, axis=1, keepdims=True) + eps)
@@ -233,8 +222,6 @@
     read_buf[kv] = jnp.concatenate(pieces, axis=1).astype(BF16)
     own_read = read_buf.at[kv]
     copies = exchange("kv", kv, n_kv, lambda p: own_read, lambda d: own_read, read_s, read_r)
-    store = pltpu.make_async_copy(next_v, new_state, store_sem.at[0])
-    store.start()
     loads[10].wait()
     for copy in copies:
         copy.wait_recv()
@@ -324,14 +311,10 @@
     for d, copy in zip(reversed(range(1, n_tp)), copies):
         copy.wait_recv()
         result += down_recv[d - 1].astype(F32)
-    mixed_v[...] = (resid_buf[tp] + result).astype(BF16)
-    last = pltpu.make_async_copy(mixed_v, mixed, store_sem.at[1])
-    last.start()
+    mixed[...] = (resid_buf[tp] + result).astype(BF16)
 
     for copy in sent:
         copy.wait_send()
-    store.wait()
-    last.wait()
 
 
 def body(n_kv, n_tp, *args):
@@ -362,7 +345,8 @@
         (i * unit, min(count, units - i) * unit) for i in range(0, units, count)
     ]
     any_spec = pl.BlockSpec(memory_space=pl.ANY)
-    sems = [pltpu.SemaphoreType.DMA((14,)), pltpu.SemaphoreType.DMA((2,))]
+    vmem = pl.BlockSpec(memory_space=pltpu.VMEM)
+    sems = [pltpu.SemaphoreType.DMA((14,))]
     for n in (
         n_tp - 1,
         4 * (n_kv - 1),
@@ -391,15 +375,11 @@
             pltpu.VMEM((batch, count), F32),
         ]
     small = [x.reshape(-1, LANES) for x in (mix_gain, lower_bound, head_gain, ffn_gain)]
-    out_shape = (
-        jax.ShapeDtypeStruct(tokens.shape, BF16),
-        jax.ShapeDtypeStruct(state.shape, F32),
-    )
     results = pl.pallas_call(
         functools.partial(kernel, n_kv, n_tp, chunks),
-        out_shape=out_shape,
+        out_shape=(pltpu.VMEM(tokens.shape, BF16), pltpu.VMEM(state.shape, F32)),
         in_specs=[any_spec] * 14,
-        out_specs=(any_spec, any_spec),
+        out_specs=(vmem, vmem),
         scratch_shapes=[
             pltpu.VMEM((4, block, width), BF16),
             pltpu.VMEM(state.shape, F32),
@@ -407,9 +387,7 @@
             pltpu.VMEM(w_gate.shape, BF16),
             pltpu.VMEM(w_up.shape, BF16),
             pltpu.VMEM(w_down.shape, BF16),
-            pltpu.VMEM(state.shape, F32),
             *[pltpu.VMEM(x.shape, x.dtype) for x in small],
-            pltpu.VMEM(tokens.shape, BF16),
             pltpu.VMEM((n_tp, batch, cols), BF16),
             pltpu.VMEM((n_kv, rows, width), BF16),
             pltpu.VMEM((batch, width), F32),
@@ -439,16 +417,14 @@
     )
     return pl.pallas_call(
         tail,
-        out_shape=out_shape,
-        in_specs=[any_spec] * 2,
+        out_shape=(
+            jax.ShapeDtypeStruct(tokens.shape, BF16),
+            jax.ShapeDtypeStruct(state.shape, F32),
+        ),
+        in_specs=[vmem] * 2,
         out_specs=(any_spec, any_spec),
-        scratch_shapes=[
-            pltpu.VMEM(tokens.shape, BF16),
-            pltpu.VMEM(state.shape, F32),
-            pltpu.SemaphoreType.DMA((1 + rows,)),
-            pltpu.SemaphoreType.DMA((1 + rows,)),
-        ],
-    )(*results)
+        scratch_shapes=[pltpu.SemaphoreType.DMA((2,))],
+    )(*[pltpu.with_memory_space_constraint(x, pltpu.VMEM) for x in results])
 
 
 def solution(mesh):

time: 39.8 us -> 38.2 us (0.960)
  Pallas kernels: 38.9 us -> 37.4 us
    pallas_call x2, Pallas kernels: 38.9 us -> 37.4 us  [the longest x1 36.4 us: body(): pl.pallas_call(functools.partial(kernel, n_kv, n_tp, chunks), out_shape=(...]
where the time goes in v3:
time: 38.2 us; the launch traced here: 38 us
  Pallas kernels  37.4 us (98%)
  between operations  0.64 us (2%)
    pallas_call x1, Pallas kernels, body(): pl.pallas_call(functools.partial(kernel, n_kv, n_tp, chunks), out_shape=(...  36.4 us
    pallas_call x1, Pallas kernels, body(): pl.pallas_call(tail, out_shape=(jax.ShapeDtypeStruct(tokens.shape, BF16),...  0.99 us

profile of v3, /device:TPU:0, one launch (start us, length us, event | category | flops | bytes accessed | tf_op | source)
XLA Modules:
  0.0 38.0 jit_solution(3337774015658272192)
XLA Ops:
  0.6 36.4 %shard_map.149 = (bf16[16,256]{1,0:T(8,128)(2,1)S(1)}, f32[4,4,128,128]{3,2,1,0:T(8,128)S(1)}) custom-call(bf16[16,256]{1,0:T(8,128)(2,1)} %tokens.1, bf16[8,128]{1,0:T(8,128)(2,1)} %bitcast.4, bf16[1024,512]{1,0:T(8,128)(2,1)} %w_query.1, bf16[1024,512]{1,0:T(8,128)(2,1)} %w_forget.1, bf16[1024,512]{1,0:T(8,128)(2,1)} %w_input.1, ...), custom_call_target="tpu_custom_call" | custom-call | tf_op jit(solution)/shard_map/pallas_call | solution.py:378
  37.0 1.0 %shard_map.150 = (bf16[16,256]{1,0:T(8,128)(2,1)}, f32[4,4,128,128]{3,2,1,0:T(8,128)}) custom-call(bf16[16,256]{1,0:T(8,128)(2,1)S(1)} %get-tuple-element.4.mixed_in, f32[4,4,128,128]{3,2,1,0:T(8,128)S(1)} %get-tuple-element.5.state_in), custom_call_target="tpu_custom_call" | custom-call | tf_op jit(solution)/shard_map/pallas_call | solution.py:418
